TPU v7x, 32 devices: a whole 2x2x4 slice. The times are simulated.
32 devices in a mesh: ep: 4 (over z), tp: 8 (over y, x, core).
Axes of the slice: x: 2, y: 2, z: 4, core: 2. Of those that a mesh axis runs over, the one named last changes fastest.
Arguments:
- tokens: bfloat16 [1024, 2048], P('ep'), may hold values from -6 to 6
- norm_gain: float32 [2048], replicated, may hold values from 0.1 to 1.9
- expert_ids: int32 [1024, 2], P('ep'), may hold values from 0 to 3, all different within a row; in each aligned block of 256 rows (0 to 255, 256 to 511, ...) at most 192 rows name the same one
- routing_weight: float32 [1024, 2], P('ep'), may hold values from 0.1 to 1
- expert_gate: bfloat16 [4, 2048, 5632], P('ep', None, 'tp'), may hold values from -0.125 to 0.125
- expert_up: bfloat16 [4, 2048, 5632], P('ep', None, 'tp'), may hold values from -0.125 to 0.125
- expert_down: bfloat16 [4, 5632, 2048], P('ep', 'tp'), may hold values from -0.078125 to 0.078125
- dense_gate_w: bfloat16 [2048, 1024], P(None, 'tp'), may hold values from -0.125 to 0.125
- dense_up_w: bfloat16 [2048, 1024], P(None, 'tp'), may hold values from -0.125 to 0.125
- dense_down_w: bfloat16 [1024, 2048], P('tp'), may hold values from -0.1875 to 0.1875
- dense_gate: float32 [2048], P('tp'), may hold values from -3 to 3
Outputs:
- layer_out: bfloat16 [1024, 2048], P('ep', 'tp')
Inputs may be any that keep to these rules, and one draw needn't show every extreme that they name: `expert_ids`: within the 256 rows of one device along ep, each row names two different experts and no expert is named by more than 192 rows; some expert is named by exactly 192 rows.
All inputs are finite; a program needn't handle non-finite values.
Results may differ from a plain program's by a relative error of at most 0.017.
Values may be sent and summed in bfloat16 or wider, within the bound.
A program may use at most 64 MiB of HBM per device.

v0:
```python
import functools
import jax
import jax.numpy as jnp
from jax import lax
from jax.experimental import pallas as pl
from jax.experimental.pallas import tpu as pltpu
from jax.sharding import PartitionSpec as P

EPSILON = 1e-06


def positions(block_ids, experts, capacity):
    flat_ids = block_ids.reshape(-1)
    one_hot = (flat_ids[:, None] == jnp.arange(experts, dtype=jnp.int32)[None, :]).astype(jnp.int32)
    earlier = jnp.cumsum(one_hot, axis=0) - one_hot
    return flat_ids * capacity + jnp.sum(earlier * one_hot, axis=1)


def transposed_term(hidden, down_w):
    return lax.dot_general(
        down_w, hidden, (((0,), (1,)), ((), ())), preferred_element_type=jnp.float32
    )


def plain_local(
    tokens,
    norm_gain,
    expert_ids,
    routing_weight,
    expert_gate,
    expert_up,
    expert_down,
    dense_gate_w,
    dense_up_w,
    dense_down_w,
    dense_gate,
):
    experts = lax.axis_size("ep")
    group_tokens, model_width = tokens.shape
    capacity = 3 * group_tokens // experts
    slots_all = experts * capacity
    part_rows = model_width // lax.axis_size("tp")
    values = tokens.astype(jnp.float32)
    factor = lax.rsqrt(jnp.mean(values * values, axis=-1, keepdims=True) + EPSILON)
    normed = (values * factor * norm_gain[None, :]).astype(jnp.bfloat16)
    places = positions(expert_ids, experts, capacity)
    token_no = jnp.arange(2 * group_tokens, dtype=jnp.int32) // 2 + 1
    sources = jnp.zeros((slots_all,), jnp.int32).at[places].set(token_no)
    padded = jnp.concatenate([jnp.zeros((1, model_width), jnp.bfloat16), normed], axis=0)
    gate_w = expert_gate[0]
    up_w = expert_up[0]
    down_w = expert_down[0]
    first_col = lax.axis_index("tp") * part_rows
    column_part = lax.dynamic_slice_in_dim(padded, first_col, part_rows, 1)
    outgoing = column_part[sources].reshape(experts, capacity, part_rows)
    landed = lax.all_to_all(outgoing, "ep", split_axis=0, concat_axis=0, tiled=True)
    portion = lax.all_gather(landed, "tp", axis=2, tiled=True)
    columns = portion.reshape(slots_all, portion.shape[2])
    gate_act = jnp.dot(columns, gate_w, preferred_element_type=jnp.float32)
    up_act = jnp.dot(columns, up_w, preferred_element_type=jnp.float32)
    hidden = (jax.nn.silu(gate_act) * up_act).astype(jnp.bfloat16)
    dense_gate_act = jnp.dot(normed, dense_gate_w, preferred_element_type=jnp.float32)
    dense_up_act = jnp.dot(normed, dense_up_w, preferred_element_type=jnp.float32)
    dense_hidden = (jax.nn.silu(dense_gate_act) * dense_up_act).astype(jnp.bfloat16)
    dense_out = lax.psum_scatter(
        transposed_term(dense_hidden, dense_down_w).astype(jnp.bfloat16),
        "tp",
        scatter_dimension=0,
        tiled=True,
    ).astype(jnp.float32)
    expert_out = lax.psum_scatter(
        transposed_term(hidden, down_w).astype(jnp.bfloat16), "tp", scatter_dimension=0, tiled=True
    )
    expert_half = expert_out.reshape(part_rows, experts, capacity)
    returned = lax.all_to_all(expert_half, "ep", split_axis=1, concat_axis=1, tiled=True).reshape(
        part_rows, slots_all
    )
    picked = (
        jnp.take(returned, places, axis=1).astype(jnp.float32).reshape(part_rows, group_tokens, 2)
    )
    routed = jnp.sum(picked * routing_weight[None, :, :], axis=2)
    gate_factor = jax.nn.sigmoid(dense_gate)[:, None]
    return (routed + gate_factor * dense_out).T.astype(jnp.bfloat16)


BF = jnp.bfloat16
F32 = jnp.float32


def silu_mul(gate_act, up_act):
    return (gate_act / (1.0 + jnp.exp(-gate_act)) * up_act).astype(BF)


def dot_t(rows, weights):
    return lax.dot_general(rows, weights, (((1,), (1,)), ((), ())), preferred_element_type=F32)


def fused_kernel(
    experts,
    tok_ref,
    gain_ref,
    ids_ref,
    rw_ref,
    gw_hbm,
    uw_hbm,
    dw_hbm,
    dg_hbm,
    du_hbm,
    dd_hbm,
    dgate_ref,
    out_ref,
    gw,
    uw,
    dw,
    dgu,
    dd,
    normed,
    slot_row,
    slot_col,
    weight_col,
    gates,
    zsend,
    xloc,
    xbuf,
    hid,
    dhid,
    part_l,
    part_c,
    r0_l,
    r0_c,
    r1a_l,
    r1b_l,
    r1a_c,
    r1b_c,
    r2a_l,
    r2b_l,
    r2a_c,
    r2b_c,
    fin,
    ret,
    total,
    wsem,
    gsem,
    zsem,
    agsem,
    rssem,
    retsem,
):
    me = lax.axis_index("ep")
    tp = lax.axis_index("tp")
    core, xx, yy = tp % 2, (tp // 2) % 2, tp // 4
    group, width = tok_ref.shape
    cols = out_ref.shape[1]
    cap = zsend.shape[1]
    ffp = gw.shape[0]
    dsp = dd.shape[0]
    rounds = experts - 1
    mesh_id = pl.DeviceIdType.MESH

    def peer(flip):
        bits = (core + flip % 2) % 2, (xx + flip // 2 % 2) % 2, (yy + flip // 4) % 2
        return bits[2] * 4 + bits[1] * 2 + bits[0]

    def ring(d):
        return lax.rem(me + d, experts)

    barrier = pltpu.get_barrier_semaphore()
    for flip in range(1, 8):
        pl.semaphore_signal(barrier, 1, device_id=(me, peer(flip)), device_id_type=mesh_id)
    for d in range(1, experts):
        pl.semaphore_signal(barrier, 1, device_id=(ring(d), tp), device_id_type=mesh_id)

    loads = [
        pltpu.make_async_copy(gw_hbm.at[0], gw, wsem.at[0]),
        pltpu.make_async_copy(uw_hbm.at[0], uw, wsem.at[1]),
        pltpu.make_async_copy(dg_hbm, dgu.at[:, pl.ds(0, dsp)], wsem.at[2]),
        pltpu.make_async_copy(du_hbm, dgu.at[:, pl.ds(dsp, dsp)], wsem.at[3]),
        pltpu.make_async_copy(dw_hbm.at[0], dw, wsem.at[4]),
        pltpu.make_async_copy(dd_hbm, dd, wsem.at[5]),
    ]
    for load in loads:
        load.start()

    gain = gain_ref[...]
    step = 32

    def norm_rows(i, carry):
        rows = pl.ds(pl.multiple_of(i * step, step), step)
        values = tok_ref[rows, :].astype(F32)
        factor = lax.rsqrt(jnp.sum(values * values, axis=1, keepdims=True) * (1.0 / width) + EPSILON)
        normed[rows, :] = (values * factor * gain).astype(BF)
        return carry

    lax.fori_loop(0, group // step, norm_rows, 0)

    id0, id1 = ids_ref[0:1, :], ids_ref[1:2, :]
    number = lax.broadcasted_iota(jnp.int32, (128, group), 0)
    named = (id0 == number) | (id1 == number)
    earlier = jnp.where(
        lax.broadcasted_iota(jnp.int32, (group, group), 0)
        < lax.broadcasted_iota(jnp.int32, (group, group), 1),
        1.0,
        0.0,
    ).astype(BF)
    marks = jnp.where(named, 1.0, 0.0).astype(BF)
    count = jnp.dot(marks, earlier, preferred_element_type=F32)
    slots = jnp.where(named, count, -1.0)
    weights = jnp.where(id0 == number, rw_ref[0:1, :], 0.0) + jnp.where(id1 == number, rw_ref[1:2, :], 0.0)
    slot_row[...] = slots
    slot_col[...] = slots.T
    weight_col[...] = weights.T
    lane = lax.broadcasted_iota(jnp.int32, (group, 128), 1)

    def pick(e):
        row = slot_row[pl.ds(e, 1), :].astype(jnp.int32)
        where = lax.broadcasted_iota(jnp.int32, (cap, group), 0)
        return jnp.where(row == where, 1.0, 0.0).astype(BF)

    def combine(e):
        slot = jnp.sum(jnp.where(lane == e, slot_col[...], 0.0), axis=1, keepdims=True).astype(jnp.int32)
        weight = jnp.sum(jnp.where(lane == e, weight_col[...], 0.0), axis=1, keepdims=True)
        where = lax.broadcasted_iota(jnp.int32, (group, cap), 1)
        full = jnp.where(slot == where, weight, 0.0)
        high = full.astype(BF)
        return high, (full - high.astype(F32)).astype(BF)

    def mix(pair, rows):
        return jnp.dot(pair[0], rows, preferred_element_type=F32) + jnp.dot(
            pair[1], rows, preferred_element_type=F32
        )

    pl.semaphore_wait(barrier, 7 + rounds)

    pending = []

    def send(src, dst, sems, index, target):
        copy = pltpu.make_async_remote_copy(
            src_ref=src,
            dst_ref=dst,
            send_sem=sems.at[(0,) + index],
            recv_sem=sems.at[(1,) + index],
            device_id=target,
            device_id_type=mesh_id,
        )
        copy.start()
        pending.append(copy)
        return copy

    def at_tp(flip):
        return (me, peer(flip))

    def span(slice_no):
        return pl.ds(pl.multiple_of(slice_no * cols, cols), cols)

    zcopies, order = {}, list(range(1, experts))
    if rounds == 3:
        order = [1, 3, 2]
    for d in order:
        rows = jnp.dot(pick(ring(d)), normed[:, span(tp)], preferred_element_type=F32)
        zsend[d - 1] = rows.astype(BF)
        zcopies[d] = send(zsend.at[d - 1], xbuf.at[d - 1, :, span(tp)], zsem, (d - 1,), (ring(d), tp))
    gcopies = [send(dgate_ref, gates.at[tp], gsem, (f - 1,), at_tp(f)) for f in range(1, 8)]
    gates[tp] = dgate_ref[...]
    here = pick(me)

    def local_rows(k, carry):
        at = pl.ds(pl.multiple_of(k * cols, cols), cols)
        xloc[:, at] = jnp.dot(here, normed[:, at], preferred_element_type=F32).astype(BF)
        return carry

    lax.fori_loop(0, width // cols, local_rows, 0)

    half = cap // 2
    top, bottom = pl.ds(0, half), pl.ds(half, half)
    everything = pl.ds(0, cap)
    ag = {}

    def move(d, name, number, rows, slice_flip, flip):
        ref = xbuf.at[d - 1, rows, span(peer(slice_flip))]
        ag[d, name] = send(ref, ref, agsem, (d - 1, number), at_tp(flip))

    def ag1(d):
        zcopies[d].wait_recv()
        move(d, "x", 0, everything, 0, 2)
        move(d, "y", 1, everything, 0, 4)
        move(d, "c", 2, everything, 0, 1)

    def ag2(d):
        ag[d, "x"].wait_recv()
        move(d, "xy", 3, top, 2, 4)
        move(d, "xc", 4, everything, 2, 1)
        ag[d, "y"].wait_recv()
        move(d, "yx", 5, bottom, 4, 2)
        move(d, "yc", 6, everything, 4, 1)

    def ag3(d):
        ag[d, "xy"].wait_recv()
        move(d, "xyc", 7, top, 6, 1)
        ag[d, "yx"].wait_recv()
        move(d, "yxc", 8, bottom, 6, 1)

    def ag_done(d):
        for name in ("c", "xc", "yc", "xyc", "yxc"):
            ag[d, name].wait_recv()

    tiles = [(n, min(256, ffp - n)) for n in range(0, ffp, 256)]

    def hidden(rows_ref):
        for n, size in tiles:
            gate_act = dot_t(rows_ref[...], gw[n : n + size, :])
            up_act = dot_t(rows_ref[...], uw[n : n + size, :])
            hid[:, n : n + size] = silu_mul(gate_act, up_act)

    def rs_refs(b):
        if b == 0:
            return part_l, r0_l, r1a_l, r1b_l, r2a_l, r2b_l
        return tuple(r.at[b - 1] for r in (part_c, r0_c, r1a_c, r1b_c, r2a_c, r2b_c))

    rs = {}

    def rs0(b):
        part, r0 = rs_refs(b)[:2]
        rs[b, 0] = send(part.at[1 - core], r0, rssem, (b, 0), at_tp(1))

    def add(dst, index, other):
        dst[index] = (dst[index].astype(F32) + other.astype(F32)).astype(BF)

    def rs1(b):
        part, r0, r1a, r1b = rs_refs(b)[:4]
        h = part.shape[3] // 2
        rs[b, 0].wait_recv()
        for q in range(4):
            add(part, (core, q // 2, q % 2), r0[q // 2, q % 2])
        rs[b, 1] = send(part.at[core, :, 1 - xx, pl.ds(0, h)], r1a, rssem, (b, 1), at_tp(2))
        rs[b, 2] = send(part.at[core, 1 - yy, :, pl.ds(h, h)], r1b, rssem, (b, 2), at_tp(4))

    def rs2(b):
        part, r0, r1a, r1b, r2a, r2b = rs_refs(b)
        h = part.shape[3] // 2
        rs[b, 1].wait_recv()
        add(part, (core, 1 - yy, xx, pl.ds(0, h)), r1a[1 - yy])
        rs[b, 3] = send(part.at[core, 1 - yy, xx, pl.ds(0, h)], r2a, rssem, (b, 3), at_tp(4))
        rs[b, 2].wait_recv()
        add(part, (core, yy, 1 - xx, pl.ds(h, h)), r1b[1 - xx])
        rs[b, 4] = send(part.at[core, yy, 1 - xx, pl.ds(h, h)], r2b, rssem, (b, 4), at_tp(2))

    def rs3(b):
        part, r0, r1a, r1b, r2a, r2b = rs_refs(b)
        h = part.shape[3] // 2
        rs[b, 3].wait_recv()
        upper = part[core, yy, xx, pl.ds(0, h)].astype(F32) + r1a[yy].astype(F32) + r2a[...].astype(F32)
        if b == 0:
            total[pl.ds(0, h), :] = upper
        else:
            fin[b - 1, pl.ds(0, h), :] = upper.astype(BF)
        rs[b, 4].wait_recv()
        lower = part[core, yy, xx, pl.ds(h, h)].astype(F32) + r1b[xx].astype(F32) + r2b[...].astype(F32)
        if b == 0:
            total[pl.ds(h, h), :] = lower
        else:
            fin[b - 1, pl.ds(h, h), :] = lower.astype(BF)
            back = lax.rem(me + experts - b, experts)
            rs[b, 5] = send(fin.at[b - 1], ret.at[b - 1], retsem, (b - 1,), (back, tp))

    def partials(b):
        part = rs_refs(b)[0]

        def one(which):
            def body(q, carry):
                at = span(2 * q + which)
                value = jnp.dot(hid[...], dw[:, at], preferred_element_type=F32)
                part[which, q // 2, q % 2] = value.astype(BF)
                return carry

            lax.fori_loop(0, 4, body, 0)

        one(1 - core)
        rs0(b)
        one(core)

    def dense_partials():
        pair = combine(me)

        def one(which):
            def body(q, carry):
                k = 2 * q + which
                at = span(k)
                value = jnp.dot(hid[...], dw[:, at], preferred_element_type=F32).astype(BF)
                side = jnp.dot(dhid[...], dd[:, at], preferred_element_type=F32)
                part_l[which, q // 2, q % 2] = (
                    mix(pair, value) + jax.nn.sigmoid(gates[k]) * side
                ).astype(BF)
                return carry

            lax.fori_loop(0, 4, body, 0)

        one(1 - core)
        rs0(0)
        one(core)

    def returned(b):
        rs[b, 5].wait_recv()
        total[...] += mix(combine(ring(b)), ret[b - 1])

    first, second, third = order
    loads[0].wait()
    loads[1].wait()
    hidden(xloc)
    ag1(first)
    loads[2].wait()
    loads[3].wait()
    acts = jnp.dot(normed[...], dgu[...], preferred_element_type=F32)
    dhid[...] = silu_mul(acts[:, :dsp], acts[:, dsp:])
    ag1(second)
    loads[4].wait()
    loads[5].wait()
    for copy in gcopies:
        copy.wait_recv()
    dense_partials()
    ag2(first)
    ag1(third)
    ag2(second)
    ag3(first)
    rs1(0)
    ag2(third)
    ag3(second)
    ag_done(first)
    hidden(xbuf.at[first - 1])
    partials(first)
    ag3(third)
    rs2(0)
    rs1(first)
    ag_done(second)
    hidden(xbuf.at[second - 1])
    partials(second)
    rs2(first)
    rs1(second)
    ag_done(third)
    hidden(xbuf.at[third - 1])
    partials(third)
    rs3(first)
    rs2(second)
    rs1(third)
    rs3(0)
    rs3(second)
    rs2(third)
    returned(first)
    returned(second)
    rs3(third)
    returned(third)
    out_ref[...] = total[...].astype(BF)
    for copy in pending:
        copy.wait_send()


def fused_local(
    tokens,
    norm_gain,
    expert_ids,
    routing_weight,
    expert_gate,
    expert_up,
    expert_down,
    dense_gate_w,
    dense_up_w,
    dense_down_w,
    dense_gate,
):
    experts = lax.axis_size("ep")
    parts = lax.axis_size("tp")
    group, width = tokens.shape
    cap = 3 * group // experts
    cols = width // parts
    ffp = expert_gate.shape[2]
    dsp = dense_gate_w.shape[1]
    rounds = experts - 1
    vmem, hbm = pl.BlockSpec(memory_space=pltpu.VMEM), pl.BlockSpec(memory_space=pl.ANY)
    dma = pltpu.SemaphoreType.DMA
    half, ghalf = cap // 2, group // 2
    return pl.pallas_call(
        functools.partial(fused_kernel, experts),
        out_shape=jax.ShapeDtypeStruct((group, cols), BF),
        in_specs=[vmem] * 4 + [hbm] * 6 + [vmem],
        out_specs=vmem,
        scratch_shapes=[
            pltpu.VMEM((ffp, width), BF),
            pltpu.VMEM((ffp, width), BF),
            pltpu.VMEM((ffp, width), BF),
            pltpu.VMEM((width, 2 * dsp), BF),
            pltpu.VMEM((dsp, width), BF),
            pltpu.VMEM((group, width), BF),
            pltpu.VMEM((128, group), F32),
            pltpu.VMEM((group, 128), F32),
            pltpu.VMEM((group, 128), F32),
            pltpu.VMEM((parts, 1, cols), F32),
            pltpu.VMEM((rounds, cap, cols), BF),
            pltpu.VMEM((cap, width), BF),
            pltpu.VMEM((rounds, cap, width), BF),
            pltpu.VMEM((cap, ffp), BF),
            pltpu.VMEM((group, dsp), BF),
            pltpu.VMEM((2, 2, 2, group, cols), BF),
            pltpu.VMEM((rounds, 2, 2, 2, cap, cols), BF),
            pltpu.VMEM((2, 2, group, cols), BF),
            pltpu.VMEM((rounds, 2, 2, cap, cols), BF),
            pltpu.VMEM((2, ghalf, cols), BF),
            pltpu.VMEM((2, ghalf, cols), BF),
            pltpu.VMEM((rounds, 2, half, cols), BF),
            pltpu.VMEM((rounds, 2, half, cols), BF),
            pltpu.VMEM((ghalf, cols), BF),
            pltpu.VMEM((ghalf, cols), BF),
            pltpu.VMEM((rounds, half, cols), BF),
            pltpu.VMEM((rounds, half, cols), BF),
            pltpu.VMEM((rounds, cap, cols), BF),
            pltpu.VMEM((rounds, cap, cols), BF),
            pltpu.VMEM((group, cols), F32),
            dma((6,)),
            dma((2, parts - 1)),
            dma((2, rounds)),
            dma((2, rounds, 9)),
            dma((2, experts, 5)),
            dma((2, rounds)),
        ],
        compiler_params=pltpu.CompilerParams(
            collective_id=0, has_side_effects=True, vmem_limit_bytes=56 * 1024 * 1024
        ),
        name="routed_layer",
    )(
        tokens,
        norm_gain[None, :],
        expert_ids.T,
        routing_weight.T,
        jnp.swapaxes(expert_gate, 1, 2),
        jnp.swapaxes(expert_up, 1, 2),
        expert_down,
        dense_gate_w,
        dense_up_w,
        dense_down_w,
        dense_gate[None, :],
    )


def local(*args):
    experts, parts = lax.axis_size("ep"), lax.axis_size("tp")
    group, width = args[0].shape
    fits = (
        experts == 4
        and parts == 8
        and width % (128 * parts) == 0
        and group % 128 == 0
        and (3 * group // experts) % 32 == 0
        and args[7].shape[1] % 128 == 0
        and args[4].shape[2] % 16 == 0
    )
    return (fused_local if fits else plain_local)(*args)


def solution(mesh):
    return jax.shard_map(
        local,
        mesh=mesh,
        in_specs=(
            P("ep", None),
            P(),
            P("ep", None),
            P("ep", None),
            P("ep", None, "tp"),
            P("ep", None, "tp"),
            P("ep", "tp", None),
            P(None, "tp"),
            P(None, "tp"),
            P("tp", None),
            P("tp"),
        ),
        out_specs=P("ep", "tp"),
        check_vma=False,
    )
```

profile of v0, /device:TPU:0, one launch (start us, length us, event | category | flops | bytes accessed | tf_op | source)
XLA Modules:
  0.0 57.8 jit_solution(17117509056812122097)
XLA Ops:
  0.0 56.2 %routed_layer.1 = bf16[256,256]{1,0:T(8,128)(2,1)} custom-call(bf16[256,2048]{1,0:T(8,128)(2,1)} %tok_ref.1, f32[1,2048]{1,0:T(1,128)} %bitcast.8, s32[2,256]{1,0:T(2,128)} %bitcast.9, f32[2,256]{1,0:T(2,128)} %bitcast.10, bf16[1,704,2048]{2,1,0:T(8,128)(2,1)} %bitcast.6, bf16[1,704,2048]{2,1,0:T(8,128)(2,1)} %bitcast.7, bf16[1,704,2048]{2,1,0:T(8,128)(2,1)} %dw_hbm.1, ...), custom_call_target="tpu_custom_call" | custom-call | tf_op jit(solution)/shard_map/routed_layer/pallas_call | solution.py:480
  56.2 1.6 %copy.13 = bf16[256,256]{1,0:T(8,128)(2,1)} copy(bf16[256,256]{1,0:T(8,128)(2,1)} %routed_layer.1) | data formatting | bytes 262144
where the time goes:
time: 57.9 us; the launch traced here: 57.8 us
  Pallas kernels  56.2 us (97%)
  local copies, waits for them, and re-layouts  1.57 us (3%)
    pallas_call x1, Pallas kernels, fused_local(): pl.pallas_call(functools.partial(fused_kernel, experts), out_shape=jax.Sh...  56.2 us
    unnamed x1, local copies, waits for them, and re-layouts  1.57 us

commit v1 on v0

v1 whole, which is shorter than its diff:
```python
import jax
import jax.numpy as jnp
from jax import lax
from jax.experimental import pallas as pl
from jax.experimental.pallas import tpu as pltpu
from jax.sharding import PartitionSpec as P

EPSILON = 1e-06


def positions(block_ids, experts, capacity):
    flat_ids = block_ids.reshape(-1)
    one_hot = (flat_ids[:, None] == jnp.arange(experts, dtype=jnp.int32)[None, :]).astype(jnp.int32)
    earlier = jnp.cumsum(one_hot, axis=0) - one_hot
    return flat_ids * capacity + jnp.sum(earlier * one_hot, axis=1)


def transposed_term(hidden, down_w):
    return lax.dot_general(
        down_w, hidden, (((0,), (1,)), ((), ())), preferred_element_type=jnp.float32
    )


def plain_local(
    tokens,
    norm_gain,
    expert_ids,
    routing_weight,
    expert_gate,
    expert_up,
    expert_down,
    dense_gate_w,
    dense_up_w,
    dense_down_w,
    dense_gate,
):
    experts = lax.axis_size("ep")
    group_tokens, model_width = tokens.shape
    capacity = 3 * group_tokens // experts
    slots_all = experts * capacity
    part_rows = model_width // lax.axis_size("tp")
    values = tokens.astype(jnp.float32)
    factor = lax.rsqrt(jnp.mean(values * values, axis=-1, keepdims=True) + EPSILON)
    normed = (values * factor * norm_gain[None, :]).astype(jnp.bfloat16)
    places = positions(expert_ids, experts, capacity)
    token_no = jnp.arange(2 * group_tokens, dtype=jnp.int32) // 2 + 1
    sources = jnp.zeros((slots_all,), jnp.int32).at[places].set(token_no)
    padded = jnp.concatenate([jnp.zeros((1, model_width), jnp.bfloat16), normed], axis=0)
    gate_w = expert_gate[0]
    up_w = expert_up[0]
    down_w = expert_down[0]
    first_col = lax.axis_index("tp") * part_rows
    column_part = lax.dynamic_slice_in_dim(padded, first_col, part_rows, 1)
    outgoing = column_part[sources].reshape(experts, capacity, part_rows)
    landed = lax.all_to_all(outgoing, "ep", split_axis=0, concat_axis=0, tiled=True)
    portion = lax.all_gather(landed, "tp", axis=2, tiled=True)
    columns = portion.reshape(slots_all, portion.shape[2])
    gate_act = jnp.dot(columns, gate_w, preferred_element_type=jnp.float32)
    up_act = jnp.dot(columns, up_w, preferred_element_type=jnp.float32)
    hidden = (jax.nn.silu(gate_act) * up_act).astype(jnp.bfloat16)
    dense_gate_act = jnp.dot(normed, dense_gate_w, preferred_element_type=jnp.float32)
    dense_up_act = jnp.dot(normed, dense_up_w, preferred_element_type=jnp.float32)
    dense_hidden = (jax.nn.silu(dense_gate_act) * dense_up_act).astype(jnp.bfloat16)
    dense_out = lax.psum_scatter(
        transposed_term(dense_hidden, dense_down_w).astype(jnp.bfloat16),
        "tp",
        scatter_dimension=0,
        tiled=True,
    ).astype(jnp.float32)
    expert_out = lax.psum_scatter(
        transposed_term(hidden, down_w).astype(jnp.bfloat16), "tp", scatter_dimension=0, tiled=True
    )
    expert_half = expert_out.reshape(part_rows, experts, capacity)
    returned = lax.all_to_all(expert_half, "ep", split_axis=1, concat_axis=1, tiled=True).reshape(
        part_rows, slots_all
    )
    picked = (
        jnp.take(returned, places, axis=1).astype(jnp.float32).reshape(part_rows, group_tokens, 2)
    )
    routed = jnp.sum(picked * routing_weight[None, :, :], axis=2)
    gate_factor = jax.nn.sigmoid(dense_gate)[:, None]
    return (routed + gate_factor * dense_out).T.astype(jnp.bfloat16)


BF = jnp.bfloat16
F32 = jnp.float32


def silu_mul(gate_act, up_act):
    return (gate_act / (1.0 + jnp.exp(-gate_act)) * up_act).astype(BF)


def dot_t(rows, weights):
    return lax.dot_general(rows, weights, (((1,), (1,)), ((), ())), preferred_element_type=F32)


ORDER = (1, 2, 3)
SCHEDULE = (
    "N", "H00", "H01", "H02", "G10", "G11", "C1", "D", "P00", "P01", "G20", "G21", "C2",
    "X1", "Y1", "S1", "G30", "G31", "C3", "A0", "X2", "Y2", "S2", "L1", "H10", "H11",
    "H12", "P10", "X3", "Y3", "S3", "P11", "L2", "E0", "F0", "A1", "H20", "H21", "H22",
    "P20", "P21", "L3", "E1", "F1", "A2", "H30", "H31", "H32", "P30", "P31", "I1", "J1",
    "E2", "F2", "A3", "I0", "J0", "I2", "J2", "E3", "F3", "R1", "R2", "I3", "J3", "R3",
)


def fused_kernel(
    tok_ref,
    gain_ref,
    ids_ref,
    rw_ref,
    gw_hbm,
    uw_hbm,
    dw_hbm,
    dg_hbm,
    du_hbm,
    dd_hbm,
    dgate_ref,
    out_ref,
    gw,
    uw,
    dw,
    dgu,
    dd,
    factor,
    normed,
    slot_row,
    slot_col,
    weight_col,
    gates,
    zsend,
    xbuf,
    hid_l,
    hid_c,
    dhid,
    part_l,
    part_c,
    r0_l,
    r0_c,
    r1a_l,
    r1b_l,
    r1a_c,
    r1b_c,
    r2a_l,
    r2b_l,
    r2a_c,
    r2b_c,
    fin,
    ret,
    total,
    wsem,
    sems,
):
    me = lax.axis_index("ep")
    tp = lax.axis_index("tp")
    core, xx, yy = tp % 2, (tp // 2) % 2, tp // 4
    group, width = tok_ref.shape
    cols = out_ref.shape[1]
    rounds, cap = zsend.shape[:2]
    ffp = gw.shape[0]
    dsp = dd.shape[0]
    half = cap // 2
    mesh_id = pl.DeviceIdType.MESH
    to_core, to_x, to_y = 1, 2, 4

    def peer(flip):
        bits = (core + flip % 2) % 2, (xx + flip // 2 % 2) % 2, (yy + flip // 4) % 2
        return bits[2] * 4 + bits[1] * 2 + bits[0]

    def partner(j):
        return (me // 2 + j // 2) % 2 * 2 + (me % 2 + j % 2) % 2

    barrier = pltpu.get_barrier_semaphore()
    for flip in range(1, 8):
        pl.semaphore_signal(barrier, 1, device_id=(me, peer(flip)), device_id_type=mesh_id)
    for j in range(1, rounds + 1):
        pl.semaphore_signal(barrier, 1, device_id=(partner(j), tp), device_id_type=mesh_id)

    loads = {
        "g": pltpu.make_async_copy(gw_hbm.at[0], gw, wsem.at[0]),
        "u": pltpu.make_async_copy(uw_hbm.at[0], uw, wsem.at[1]),
        "dg": pltpu.make_async_copy(dg_hbm, dgu.at[:, pl.ds(0, dsp)], wsem.at[2]),
        "du": pltpu.make_async_copy(du_hbm, dgu.at[:, pl.ds(dsp, dsp)], wsem.at[3]),
        "d": pltpu.make_async_copy(dw_hbm.at[0], dw, wsem.at[4]),
        "dd": pltpu.make_async_copy(dd_hbm, dd, wsem.at[5]),
    }
    for load in loads.values():
        load.start()

    def need(*names):
        for name in names:
            if name in loads:
                loads.pop(name).wait()

    sent, arrived = {}, set()

    def send(name, src, dst, target):
        n = len(sent)
        copy = pltpu.make_async_remote_copy(
            src_ref=src,
            dst_ref=dst,
            send_sem=sems.at[0, n],
            recv_sem=sems.at[1, n],
            device_id=target,
            device_id_type=mesh_id,
        )
        copy.start()
        sent[name] = copy

    def got(*names):
        for name in names:
            if name not in arrived:
                sent[name].wait_recv()
                arrived.add(name)

    def at_tp(flip):
        return (me, peer(flip))

    def span(slice_no):
        return pl.ds(pl.multiple_of(slice_no * cols, cols), cols)

    step = 64
    for i in range(0, group, step):
        values = tok_ref[i : i + step, :].astype(F32)
        mean = jnp.sum(values * values, axis=1, keepdims=True) * (1.0 / width)
        factor[i : i + step, :] = jnp.broadcast_to(lax.rsqrt(mean + EPSILON), (step, 128))

    id0, id1 = ids_ref[0:1, :], ids_ref[1:2, :]
    number = lax.broadcasted_iota(jnp.int32, (128, group), 0)
    named = (id0 == number) | (id1 == number)
    earlier = jnp.where(
        lax.broadcasted_iota(jnp.int32, (group, group), 0)
        < lax.broadcasted_iota(jnp.int32, (group, group), 1),
        1.0,
        0.0,
    ).astype(BF)
    marks = jnp.where(named, 1.0, 0.0).astype(BF)
    count = jnp.dot(marks, earlier, preferred_element_type=F32)
    slots = jnp.where(named, count, -1.0)
    slot_row[...] = slots

    def pick(e):
        row = slot_row[pl.ds(e, 1), :].astype(jnp.int32)
        where = lax.broadcasted_iota(jnp.int32, (cap, group), 0)
        return jnp.where(row == where, 1.0, 0.0).astype(BF)

    own = (tok_ref[:, span(tp)].astype(F32) * factor[:, 0:1] * gain_ref[:, span(tp)]).astype(BF)
    tops = {0: pl.ds(0, half), 1: pl.ds(half, half)}
    gates[tp] = dgate_ref[...]
    for n, j in enumerate(ORDER):
        zsend[j - 1] = jnp.dot(pick(partner(j)), own, preferred_element_type=F32).astype(BF)
        if n == 0:
            pl.semaphore_wait(barrier, 7 + rounds)
        for h, rows in tops.items():
            send(("z", j, h), zsend.at[j - 1, rows], xbuf.at[j - 1, rows, span(tp)], (partner(j), tp))
    for flip in range(1, 8):
        send(("gate", flip), dgate_ref, gates.at[tp], at_tp(flip))

    weights = jnp.where(id0 == number, rw_ref[0:1, :], 0.0) + jnp.where(id1 == number, rw_ref[1:2, :], 0.0)
    slot_col[...] = slots.T
    weight_col[...] = weights.T
    lane = lax.broadcasted_iota(jnp.int32, (group, 128), 1)

    def weight_of(e):
        return jnp.sum(jnp.where(lane == e, weight_col[...], 0.0), axis=1, keepdims=True)

    def norm_all():
        gain = gain_ref[...]

        def body(i, carry):
            rows = pl.ds(pl.multiple_of(i * 32, 32), 32)
            values = tok_ref[rows, :].astype(F32)
            normed[rows, :] = (values * factor[rows, 0:1] * gain).astype(BF)
            return carry

        lax.fori_loop(0, group // 32, body, 0)

    def forward(name, j, rows, slice_flip, flip):
        ref = xbuf.at[j - 1, rows, span(peer(slice_flip))]
        send((name, j), ref, ref, at_tp(flip))

    everything = pl.ds(0, cap)

    def gather_start(j, h):
        got(("z", j, h))
        forward("x%d" % h, j, tops[h], 0, to_x)
        forward("y%d" % h, j, tops[h], 0, to_y)

    def gather_core(j):
        forward("c", j, everything, 0, to_core)

    def gather_relay_x(j):
        got(("x0", j))
        forward("xy", j, tops[0], to_x, to_y)

    def gather_relay_y(j):
        got(("y1", j))
        forward("yx", j, tops[1], to_y, to_x)

    def gather_share(j):
        got(("x0", j), ("x1", j))
        forward("xc", j, everything, to_x, to_core)
        got(("y0", j), ("y1", j))
        forward("yc", j, everything, to_y, to_core)

    def gather_last(j):
        got(("xy", j))
        forward("xyc", j, tops[0], to_x + to_y, to_core)
        got(("yx", j))
        forward("yxc", j, tops[1], to_x + to_y, to_core)

    tiles = [(n, min(256, ffp - n)) for n in range(0, ffp, 256)]

    def hidden_tile(b, t):
        need("g", "u")
        if b:
            got(*[(name, b) for name in ("c", "xc", "yc", "xyc", "yxc")])
        rows = xbuf[b - 1] if b else normed[...]
        n, size = tiles[t]
        value = silu_mul(dot_t(rows, gw[n : n + size, :]), dot_t(rows, uw[n : n + size, :]))
        if b:
            hid_c[b - 1, :, n : n + size] = value
        else:
            hid_l[:, n : n + size] = value

    def dense_hidden():
        need("dg", "du")
        acts = jnp.dot(normed[...], dgu[...], preferred_element_type=F32)
        dhid[...] = silu_mul(acts[:, :dsp], acts[:, dsp:])

    def rs_refs(b):
        if b == 0:
            return part_l, r0_l, r1a_l, r1b_l, r2a_l, r2b_l
        return tuple(r.at[b - 1] for r in (part_c, r0_c, r1a_c, r1b_c, r2a_c, r2b_c))

    def halves(b):
        h = (cap if b else group) // 2
        return pl.ds(0, h), pl.ds(h, h)

    def partial(b, mine):
        need("d", "dd")
        which = core if mine else 1 - core
        part, r0 = rs_refs(b)[:2]
        if b == 0:
            scale = weight_of(me)
            got(*[("gate", flip) for flip in range(1, 8)])
        for q in range(4):
            k = 2 * q + which
            if b:
                value = jnp.dot(hid_c[b - 1], dw[:, span(k)], preferred_element_type=F32)
            else:
                side = jnp.dot(dhid[...], dd[:, span(k)], preferred_element_type=F32)
                value = jnp.dot(hid_l[...], dw[:, span(k)], preferred_element_type=F32)
                value = scale * value + jax.nn.sigmoid(gates[k]) * side
            part[which, q // 2, q % 2] = value.astype(BF)
        if not mine:
            send(("r0", b), part.at[1 - core], r0, at_tp(to_core))

    def add(dst, index, other):
        dst[index] = (dst[index].astype(F32) + other.astype(F32)).astype(BF)

    def scatter_one(b):
        part, r0, r1a, r1b = rs_refs(b)[:4]
        top, bottom = halves(b)
        got(("r0", b))
        add(part, (core, 1 - yy, 1 - xx), r0[1 - yy, 1 - xx])
        send(("a0", b), part.at[core, 1 - yy, 1 - xx, top], r1a.at[1 - yy], at_tp(to_x))
        send(("b0", b), part.at[core, 1 - yy, 1 - xx, bottom], r1b.at[1 - xx], at_tp(to_y))
        add(part, (core, yy, 1 - xx), r0[yy, 1 - xx])
        send(("a1", b), part.at[core, yy, 1 - xx, top], r1a.at[yy], at_tp(to_x))
        add(part, (core, 1 - yy, xx), r0[1 - yy, xx])
        send(("b1", b), part.at[core, 1 - yy, xx, bottom], r1b.at[xx], at_tp(to_y))
        add(part, (core, yy, xx), r0[yy, xx])

    def scatter_two_a(b):
        part, r0, r1a, r1b, r2a, r2b = rs_refs(b)
        top, bottom = halves(b)
        got(("a0", b))
        add(part, (core, 1 - yy, xx, top), r1a[1 - yy])
        send(("a2", b), part.at[core, 1 - yy, xx, top], r2a, at_tp(to_y))

    def scatter_two_b(b):
        part, r0, r1a, r1b, r2a, r2b = rs_refs(b)
        top, bottom = halves(b)
        got(("b0", b))
        add(part, (core, yy, 1 - xx, bottom), r1b[1 - xx])
        send(("b2", b), part.at[core, yy, 1 - xx, bottom], r2b, at_tp(to_x))

    def finish(b, h, value):
        rows = halves(b)[h]
        if b == 0:
            total[rows, :] = value
        else:
            fin[b - 1, rows, :] = value.astype(BF)
            send(("ret", b, h), fin.at[b - 1, rows], ret.at[b - 1, rows], (partner(b), tp))

    def scatter_three_a(b):
        part, r0, r1a, r1b, r2a, r2b = rs_refs(b)
        got(("a1", b), ("a2", b))
        mine = part[core, yy, xx, halves(b)[0]].astype(F32)
        finish(b, 0, mine + r1a[yy].astype(F32) + r2a[...].astype(F32))

    def scatter_three_b(b):
        part, r0, r1a, r1b, r2a, r2b = rs_refs(b)
        got(("b1", b), ("b2", b))
        mine = part[core, yy, xx, halves(b)[1]].astype(F32)
        finish(b, 1, mine + r1b[xx].astype(F32) + r2b[...].astype(F32))

    def returned(j):
        e = partner(j)
        slot = jnp.sum(jnp.where(lane == e, slot_col[...], 0.0), axis=1, keepdims=True).astype(jnp.int32)
        place = jnp.where(slot == lax.broadcasted_iota(jnp.int32, (group, cap), 1), 1.0, 0.0).astype(BF)
        scale = weight_of(e)
        got(("ret", j, 0), ("ret", j, 1))
        total[...] += scale * jnp.dot(place, ret[j - 1], preferred_element_type=F32)

    steps = {
        "N": norm_all,
        "G": gather_start,
        "C": gather_core,
        "X": gather_relay_x,
        "Y": gather_relay_y,
        "S": gather_share,
        "L": gather_last,
        "H": hidden_tile,
        "D": dense_hidden,
        "P": partial,
        "A": scatter_one,
        "E": scatter_two_a,
        "F": scatter_two_b,
        "I": scatter_three_a,
        "J": scatter_three_b,
        "R": returned,
    }
    for word in SCHEDULE:
        steps[word[0]](*[int(digit) for digit in word[1:]])
    out_ref[...] = total[...].astype(BF)
    for copy in sent.values():
        copy.wait_send()


def fused_local(
    tokens,
    norm_gain,
    expert_ids,
    routing_weight,
    expert_gate,
    expert_up,
    expert_down,
    dense_gate_w,
    dense_up_w,
    dense_down_w,
    dense_gate,
):
    experts = lax.axis_size("ep")
    parts = lax.axis_size("tp")
    group, width = tokens.shape
    cap = 3 * group // experts
    cols = width // parts
    ffp = expert_gate.shape[2]
    dsp = dense_gate_w.shape[1]
    rounds = experts - 1
    vmem, hbm = pl.BlockSpec(memory_space=pltpu.VMEM), pl.BlockSpec(memory_space=pl.ANY)
    dma = pltpu.SemaphoreType.DMA
    half, ghalf = cap // 2, group // 2
    return pl.pallas_call(
        fused_kernel,
        out_shape=jax.ShapeDtypeStruct((group, cols), BF),
        in_specs=[vmem] * 4 + [hbm] * 6 + [vmem],
        out_specs=vmem,
        scratch_shapes=[
            pltpu.VMEM((ffp, width), BF),
            pltpu.VMEM((ffp, width), BF),
            pltpu.VMEM((ffp, width), BF),
            pltpu.VMEM((width, 2 * dsp), BF),
            pltpu.VMEM((dsp, width), BF),
            pltpu.VMEM((group, 128), F32),
            pltpu.VMEM((group, width), BF),
            pltpu.VMEM((128, group), F32),
            pltpu.VMEM((group, 128), F32),
            pltpu.VMEM((group, 128), F32),
            pltpu.VMEM((parts, 1, cols), F32),
            pltpu.VMEM((rounds, cap, cols), BF),
            pltpu.VMEM((rounds, cap, width), BF),
            pltpu.VMEM((group, ffp), BF),
            pltpu.VMEM((rounds, cap, ffp), BF),
            pltpu.VMEM((group, dsp), BF),
            pltpu.VMEM((2, 2, 2, group, cols), BF),
            pltpu.VMEM((rounds, 2, 2, 2, cap, cols), BF),
            pltpu.VMEM((2, 2, group, cols), BF),
            pltpu.VMEM((rounds, 2, 2, cap, cols), BF),
            pltpu.VMEM((2, ghalf, cols), BF),
            pltpu.VMEM((2, ghalf, cols), BF),
            pltpu.VMEM((rounds, 2, half, cols), BF),
            pltpu.VMEM((rounds, 2, half, cols), BF),
            pltpu.VMEM((ghalf, cols), BF),
            pltpu.VMEM((ghalf, cols), BF),
            pltpu.VMEM((rounds, half, cols), BF),
            pltpu.VMEM((rounds, half, cols), BF),
            pltpu.VMEM((rounds, cap, cols), BF),
            pltpu.VMEM((rounds, cap, cols), BF),
            pltpu.VMEM((group, cols), F32),
            dma((6,)),
            dma((2, 84)),
        ],
        compiler_params=pltpu.CompilerParams(
            collective_id=0, has_side_effects=True, vmem_limit_bytes=56 * 1024 * 1024
        ),
        name="routed_layer",
    )(
        tokens,
        norm_gain[None, :],
        expert_ids.T,
        routing_weight.T,
        jnp.swapaxes(expert_gate, 1, 2),
        jnp.swapaxes(expert_up, 1, 2),
        expert_down,
        dense_gate_w,
        dense_up_w,
        dense_down_w,
        dense_gate[None, :],
    )


def local(*args):
    experts, parts = lax.axis_size("ep"), lax.axis_size("tp")
    group, width = args[0].shape
    fits = (
        experts == 4
        and parts == 8
        and width % (128 * parts) == 0
        and group % 128 == 0
        and (3 * group // experts) % 32 == 0
        and args[7].shape[1] % 128 == 0
        and args[4].shape[2] % 16 == 0
    )
    return (fused_local if fits else plain_local)(*args)


def solution(mesh):
    return jax.shard_map(
        local,
        mesh=mesh,
        in_specs=(
            P("ep", None),
            P(),
            P("ep", None),
            P("ep", None),
            P("ep", None, "tp"),
            P("ep", None, "tp"),
            P("ep", "tp", None),
            P(None, "tp"),
            P(None, "tp"),
            P("tp", None),
            P("tp"),
        ),
        out_specs=P("ep", "tp"),
        check_vma=False,
    )
```

time: 57.9 us -> 50.3 us (0.87)
  Pallas kernels: 56.2 us -> 48.6 us
    pallas_call x1, Pallas kernels: 56.2 us -> 48.6 us  [fused_local(): pl.pallas_call(fused_kernel, out_shape=jax.ShapeDtypeStruct((group, cols)...]
where the time goes in v1:
time: 50.3 us; the launch traced here: 50.2 us
  Pallas kernels  48.6 us (97%)
  local copies, waits for them, and re-layouts  1.57 us (3%)
    pallas_call x1, Pallas kernels, fused_local(): pl.pallas_call(fused_kernel, out_shape=jax.ShapeDtypeStruct((group, cols)...  48.6 us
    unnamed x1, local copies, waits for them, and re-layouts  1.57 us

profile of v1, /device:TPU:0, one launch (start us, length us, event | category | flops | bytes accessed | tf_op | source)
XLA Modules:
  0.0 50.2 jit_solution(17687864442735171135)
XLA Ops:
  0.0 48.6 %routed_layer.1 = bf16[256,256]{1,0:T(8,128)(2,1)} custom-call(bf16[256,2048]{1,0:T(8,128)(2,1)} %tok_ref.1, f32[1,2048]{1,0:T(1,128)} %bitcast.8, s32[2,256]{1,0:T(2,128)} %bitcast.9, f32[2,256]{1,0:T(2,128)} %bitcast.10, bf16[1,704,2048]{2,1,0:T(8,128)(2,1)} %bitcast.6, bf16[1,704,2048]{2,1,0:T(8,128)(2,1)} %bitcast.7, bf16[1,704,2048]{2,1,0:T(8,128)(2,1)} %dw_hbm.1, ...), custom_call_target="tpu_custom_call" | custom-call | tf_op jit(solution)/shard_map/routed_layer/pallas_call | solution.py:466
  48.6 1.6 %copy.13 = bf16[256,256]{1,0:T(8,128)(2,1)} copy(bf16[256,256]{1,0:T(8,128)(2,1)} %routed_layer.1) | data formatting | bytes 262144

commit v2 on v1

--- a/solution.py
+++ b/solution.py
@@ -94,13 +94,15 @@
     return lax.dot_general(rows, weights, (((1,), (1,)), ((), ())), preferred_element_type=F32)
 
 
-ORDER = (1, 2, 3)
+SOURCES = ((3, 2, 1), (0, 3, 2), (3, 0, 1), (0, 1, 2))
+TARGETS = ((3, 1, 2), (0, 3, 2), (3, 0, 1), (0, 2, 1))
 SCHEDULE = (
-    "N", "H00", "H01", "H02", "G10", "G11", "C1", "D", "P00", "P01", "G20", "G21", "C2",
-    "X1", "Y1", "S1", "G30", "G31", "C3", "A0", "X2", "Y2", "S2", "L1", "H10", "H11",
-    "H12", "P10", "X3", "Y3", "S3", "P11", "L2", "E0", "F0", "A1", "H20", "H21", "H22",
-    "P20", "P21", "L3", "E1", "F1", "A2", "H30", "H31", "H32", "P30", "P31", "I1", "J1",
-    "E2", "F2", "A3", "I0", "J0", "I2", "J2", "E3", "F3", "R1", "R2", "I3", "J3", "R3",
+    "N", "G10", "H01", "G11", "D", "G20", "H00", "G21", "H02", "Y1", "C1", "X1", "G31",
+    "S1", "G30", "X2", "C2", "P00", "Y2", "L1", "P01", "A00", "C3", "H12", "Y3", "H10",
+    "S2", "X3", "H11", "L2", "A01", "S3", "P10", "P11", "H22", "A10", "H21", "A11",
+    "F0", "L3", "H20", "E0", "P20", "H30", "E1", "P21", "A20", "H32", "A21", "H31",
+    "P30", "F1", "P31", "J0", "I1", "E2", "A30", "F2", "A31", "J1", "I0", "E3", "I2",
+    "F3", "J2", "I3", "J3", "R1", "R2", "R3",
 )
 
 
@@ -149,6 +151,8 @@
     ret,
     total,
     wsem,
+    zsem,
+    rsem,
     sems,
 ):
     me = lax.axis_index("ep")
@@ -167,14 +171,24 @@
         bits = (core + flip % 2) % 2, (xx + flip // 2 % 2) % 2, (yy + flip // 4) % 2
         return bits[2] * 4 + bits[1] * 2 + bits[0]
 
-    def partner(j):
-        return (me // 2 + j // 2) % 2 * 2 + (me % 2 + j % 2) % 2
+    place_value = (1 + 3 * (me % 2)) * (1 + 15 * (me // 2))
+
+    def lookup(row):
+        return sum(value * 4**plane for plane, value in enumerate(row)) // place_value % 4
+
+    def source(slot):
+        return lookup([row[slot - 1] for row in SOURCES])
+
+    def slot_at(other):
+        return lookup([SOURCES[q].index(p) for p, q in enumerate(other)])
 
     barrier = pltpu.get_barrier_semaphore()
     for flip in range(1, 8):
         pl.semaphore_signal(barrier, 1, device_id=(me, peer(flip)), device_id_type=mesh_id)
     for j in range(1, rounds + 1):
-        pl.semaphore_signal(barrier, 1, device_id=(partner(j), tp), device_id_type=mesh_id)
+        pl.semaphore_signal(
+            barrier, 1, device_id=((me + j) % 4, peer(to_core)), device_id_type=mesh_id
+        )
 
     loads = {
         "g": pltpu.make_async_copy(gw_hbm.at[0], gw, wsem.at[0]),
@@ -192,29 +206,53 @@
             if name in loads:
                 loads.pop(name).wait()
 
-    sent, arrived = {}, set()
-
-    def send(name, src, dst, target):
-        n = len(sent)
-        copy = pltpu.make_async_remote_copy(
+    started, expected = [], {}
+
+    def transfer(src, dst, send_sem, recv_sem, target):
+        return pltpu.make_async_remote_copy(
             src_ref=src,
             dst_ref=dst,
-            send_sem=sems.at[0, n],
-            recv_sem=sems.at[1, n],
+            send_sem=send_sem,
+            recv_sem=recv_sem,
             device_id=target,
             device_id_type=mesh_id,
         )
+
+    def send(name, src, dst, target):
+        n = len(started)
+        copy = transfer(src, dst, sems.at[0, n], sems.at[1, n], target)
         copy.start()
-        sent[name] = copy
+        started.append(copy)
+        expected[name] = copy
 
     def got(*names):
         for name in names:
-            if name not in arrived:
-                sent[name].wait_recv()
-                arrived.add(name)
+            if expected[name] is not None:
+                expected[name].wait_recv()
+                expected[name] = None
+
+    def hop(sem, src, dst, number, landing, h, plane):
+        rows = tops[h]
+        copy = transfer(
+            src.at[number, rows],
+            dst(landing, rows, tp),
+            sem.at[0, number, h],
+            sem.at[1, landing, h],
+            (plane, peer(to_core)),
+        )
+        copy.start()
+        started.append(copy)
+
+    def z_place(slot, rows, part):
+        return xbuf.at[slot, rows, span(part)]
+
+    def r_place(slot, rows, part):
+        return ret.at[slot, rows]
 
     def at_tp(flip):
         return (me, peer(flip))
+
+    tops = {0: pl.ds(0, half), 1: pl.ds(half, half)}
 
     def span(slice_no):
         return pl.ds(pl.multiple_of(slice_no * cols, cols), cols)
@@ -245,14 +283,22 @@
         return jnp.where(row == where, 1.0, 0.0).astype(BF)
 
     own = (tok_ref[:, span(tp)].astype(F32) * factor[:, 0:1] * gain_ref[:, span(tp)]).astype(BF)
-    tops = {0: pl.ds(0, half), 1: pl.ds(half, half)}
     gates[tp] = dgate_ref[...]
-    for n, j in enumerate(ORDER):
-        zsend[j - 1] = jnp.dot(pick(partner(j)), own, preferred_element_type=F32).astype(BF)
+    for n in range(rounds):
+        targets = [row[n] for row in TARGETS]
+        plane = lookup(targets)
+        zsend[n] = jnp.dot(pick(plane), own, preferred_element_type=F32).astype(BF)
         if n == 0:
             pl.semaphore_wait(barrier, 7 + rounds)
+        for h in tops:
+            hop(zsem, zsend, z_place, n, slot_at(targets), h, plane)
+    for n in range(rounds):
         for h, rows in tops.items():
-            send(("z", j, h), zsend.at[j - 1, rows], xbuf.at[j - 1, rows, span(tp)], (partner(j), tp))
+            for kind, sem, src, place in (("z", zsem, zsend, z_place), ("r", rsem, fin, r_place)):
+                landed = place(n, rows, peer(to_core))
+                expected[kind, n + 1, h] = transfer(
+                    src.at[n, rows], landed, sem.at[0, n, h], sem.at[1, n, h], at_tp(to_core)
+                )
     for flip in range(1, 8):
         send(("gate", flip), dgate_ref, gates.at[tp], at_tp(flip))
 
@@ -283,19 +329,19 @@
 
     def gather_start(j, h):
         got(("z", j, h))
-        forward("x%d" % h, j, tops[h], 0, to_x)
-        forward("y%d" % h, j, tops[h], 0, to_y)
+        forward("x%d" % h, j, tops[h], to_core, to_x + to_core)
+        forward("y%d" % h, j, tops[h], to_core, to_y + to_core)
 
     def gather_core(j):
-        forward("c", j, everything, 0, to_core)
+        forward("c", j, everything, to_core, to_core)
 
     def gather_relay_x(j):
         got(("x0", j))
-        forward("xy", j, tops[0], to_x, to_y)
+        forward("xy", j, tops[0], to_x, to_y + to_core)
 
     def gather_relay_y(j):
         got(("y1", j))
-        forward("yx", j, tops[1], to_y, to_x)
+        forward("yx", j, tops[1], to_y, to_x + to_core)
 
     def gather_share(j):
         got(("x0", j), ("x1", j))
@@ -305,9 +351,9 @@
 
     def gather_last(j):
         got(("xy", j))
-        forward("xyc", j, tops[0], to_x + to_y, to_core)
+        forward("xyc", j, tops[0], 7, to_core)
         got(("yx", j))
-        forward("yxc", j, tops[1], to_x + to_y, to_core)
+        forward("yxc", j, tops[1], 7, to_core)
 
     tiles = [(n, min(256, ffp - n)) for n in range(0, ffp, 256)]
 
@@ -339,52 +385,58 @@
 
     def partial(b, mine):
         need("d", "dd")
-        which = core if mine else 1 - core
+        half_no = 0 if mine else 1
+        swap = half_no + (1 if b else 0)
         part, r0 = rs_refs(b)[:2]
         if b == 0:
             scale = weight_of(me)
             got(*[("gate", flip) for flip in range(1, 8)])
-        for q in range(4):
-            k = 2 * q + which
+        corners = ((1 - yy, 1 - xx), (yy, 1 - xx), (1 - yy, xx), (yy, xx))
+        for (y, x), odd in zip(corners, (0, 1, 1, 0)):
+            k = 4 * y + 2 * x + (core + odd + swap) % 2
             if b:
                 value = jnp.dot(hid_c[b - 1], dw[:, span(k)], preferred_element_type=F32)
             else:
                 side = jnp.dot(dhid[...], dd[:, span(k)], preferred_element_type=F32)
                 value = jnp.dot(hid_l[...], dw[:, span(k)], preferred_element_type=F32)
                 value = scale * value + jax.nn.sigmoid(gates[k]) * side
-            part[which, q // 2, q % 2] = value.astype(BF)
+            part[half_no, y, x] = value.astype(BF)
         if not mine:
-            send(("r0", b), part.at[1 - core], r0, at_tp(to_core))
+            for q, (y, x) in enumerate(corners):
+                send(("r0", q, b), part.at[half_no, y, x], r0.at[y, x], at_tp(to_core))
 
     def add(dst, index, other):
         dst[index] = (dst[index].astype(F32) + other.astype(F32)).astype(BF)
 
-    def scatter_one(b):
+    def scatter_one(b, late):
         part, r0, r1a, r1b = rs_refs(b)[:4]
         top, bottom = halves(b)
-        got(("r0", b))
-        add(part, (core, 1 - yy, 1 - xx), r0[1 - yy, 1 - xx])
-        send(("a0", b), part.at[core, 1 - yy, 1 - xx, top], r1a.at[1 - yy], at_tp(to_x))
-        send(("b0", b), part.at[core, 1 - yy, 1 - xx, bottom], r1b.at[1 - xx], at_tp(to_y))
-        add(part, (core, yy, 1 - xx), r0[yy, 1 - xx])
-        send(("a1", b), part.at[core, yy, 1 - xx, top], r1a.at[yy], at_tp(to_x))
-        add(part, (core, 1 - yy, xx), r0[1 - yy, xx])
-        send(("b1", b), part.at[core, 1 - yy, xx, bottom], r1b.at[xx], at_tp(to_y))
-        add(part, (core, yy, xx), r0[yy, xx])
+        if not late:
+            got(("r0", 0, b))
+            add(part, (0, 1 - yy, 1 - xx), r0[1 - yy, 1 - xx])
+            send(("a0", b), part.at[0, 1 - yy, 1 - xx, top], r1a.at[1 - yy], at_tp(to_x + to_core))
+            send(("b0", b), part.at[0, 1 - yy, 1 - xx, bottom], r1b.at[1 - xx], at_tp(to_y + to_core))
+        else:
+            got(("r0", 1, b))
+            add(part, (0, yy, 1 - xx), r0[yy, 1 - xx])
+            send(("a1", b), part.at[0, yy, 1 - xx, top], r1a.at[yy], at_tp(to_x + to_core))
+            got(("r0", 2, b))
+            add(part, (0, 1 - yy, xx), r0[1 - yy, xx])
+            send(("b1", b), part.at[0, 1 - yy, xx, bottom], r1b.at[xx], at_tp(to_y + to_core))
 
     def scatter_two_a(b):
         part, r0, r1a, r1b, r2a, r2b = rs_refs(b)
         top, bottom = halves(b)
         got(("a0", b))
-        add(part, (core, 1 - yy, xx, top), r1a[1 - yy])
-        send(("a2", b), part.at[core, 1 - yy, xx, top], r2a, at_tp(to_y))
+        add(part, (0, 1 - yy, xx, top), r1a[1 - yy])
+        send(("a2", b), part.at[0, 1 - yy, xx, top], r2a, at_tp(to_y + to_core))
 
     def scatter_two_b(b):
         part, r0, r1a, r1b, r2a, r2b = rs_refs(b)
         top, bottom = halves(b)
         got(("b0", b))
-        add(part, (core, yy, 1 - xx, bottom), r1b[1 - xx])
-        send(("b2", b), part.at[core, yy, 1 - xx, bottom], r2b, at_tp(to_x))
+        add(part, (0, yy, 1 - xx, bottom), r1b[1 - xx])
+        send(("b2", b), part.at[0, yy, 1 - xx, bottom], r2b, at_tp(to_x + to_core))
 
     def finish(b, h, value):
         rows = halves(b)[h]
@@ -392,26 +444,29 @@
             total[rows, :] = value
         else:
             fin[b - 1, rows, :] = value.astype(BF)
-            send(("ret", b, h), fin.at[b - 1, rows], ret.at[b - 1, rows], (partner(b), tp))
+            sources = [row[b - 1] for row in SOURCES]
+            hop(rsem, fin, r_place, b - 1, slot_at(sources), h, source(b))
 
     def scatter_three_a(b):
         part, r0, r1a, r1b, r2a, r2b = rs_refs(b)
-        got(("a1", b), ("a2", b))
-        mine = part[core, yy, xx, halves(b)[0]].astype(F32)
+        rows = halves(b)[0]
+        got(("r0", 3, b), ("a1", b), ("a2", b))
+        mine = part[0, yy, xx, rows].astype(F32) + r0[yy, xx, rows].astype(F32)
         finish(b, 0, mine + r1a[yy].astype(F32) + r2a[...].astype(F32))
 
     def scatter_three_b(b):
         part, r0, r1a, r1b, r2a, r2b = rs_refs(b)
-        got(("b1", b), ("b2", b))
-        mine = part[core, yy, xx, halves(b)[1]].astype(F32)
+        rows = halves(b)[1]
+        got(("r0", 3, b), ("b1", b), ("b2", b))
+        mine = part[0, yy, xx, rows].astype(F32) + r0[yy, xx, rows].astype(F32)
         finish(b, 1, mine + r1b[xx].astype(F32) + r2b[...].astype(F32))
 
     def returned(j):
-        e = partner(j)
+        e = source(j)
         slot = jnp.sum(jnp.where(lane == e, slot_col[...], 0.0), axis=1, keepdims=True).astype(jnp.int32)
         place = jnp.where(slot == lax.broadcasted_iota(jnp.int32, (group, cap), 1), 1.0, 0.0).astype(BF)
         scale = weight_of(e)
-        got(("ret", j, 0), ("ret", j, 1))
+        got(("r", j, 0), ("r", j, 1))
         total[...] += scale * jnp.dot(place, ret[j - 1], preferred_element_type=F32)
 
     steps = {
@@ -435,7 +490,7 @@
     for word in SCHEDULE:
         steps[word[0]](*[int(digit) for digit in word[1:]])
     out_ref[...] = total[...].astype(BF)
-    for copy in sent.values():
+    for copy in started:
         copy.wait_send()
 
 
@@ -501,7 +556,9 @@
             pltpu.VMEM((rounds, cap, cols), BF),
             pltpu.VMEM((group, cols), F32),
             dma((6,)),
-            dma((2, 84)),
+            dma((2, rounds, 2)),
+            dma((2, rounds, 2)),
+            dma((2, 92)),
         ],
         compiler_params=pltpu.CompilerParams(
             collective_id=0, has_side_effects=True, vmem_limit_bytes=56 * 1024 * 1024

time: 50.3 us -> 46.6 us (0.926)
  Pallas kernels: 48.6 us -> 44.9 us
    pallas_call x1, Pallas kernels: 48.6 us -> 44.9 us  [fused_local(): pl.pallas_call(fused_kernel, out_shape=jax.ShapeDtypeStruct((group, cols)...]
where the time goes in v2:
time: 46.6 us; the launch traced here: 46.5 us
  Pallas kernels  44.9 us (96%)
  local copies, waits for them, and re-layouts  1.57 us (3%)
    pallas_call x1, Pallas kernels, fused_local(): pl.pallas_call(fused_kernel, out_shape=jax.ShapeDtypeStruct((group, cols)...  44.9 us
    unnamed x1, local copies, waits for them, and re-layouts  1.57 us

profile of v2, /device:TPU:0, one launch (start us, length us, event | category | flops | bytes accessed | tf_op | source)
XLA Modules:
  0.0 46.5 jit_solution(5730851381062891203)
XLA Ops:
  0.0 44.9 %routed_layer.1 = bf16[256,256]{1,0:T(8,128)(2,1)} custom-call(bf16[256,2048]{1,0:T(8,128)(2,1)} %tok_ref.1, f32[1,2048]{1,0:T(1,128)} %bitcast.8, s32[2,256]{1,0:T(2,128)} %bitcast.9, f32[2,256]{1,0:T(2,128)} %bitcast.10, bf16[1,704,2048]{2,1,0:T(8,128)(2,1)} %bitcast.6, bf16[1,704,2048]{2,1,0:T(8,128)(2,1)} %bitcast.7, bf16[1,704,2048]{2,1,0:T(8,128)(2,1)} %dw_hbm.1, ...), custom_call_target="tpu_custom_call" | custom-call | tf_op jit(solution)/shard_map/routed_layer/pallas_call | solution.py:521
  44.9 1.6 %copy.13 = bf16[256,256]{1,0:T(8,128)(2,1)} copy(bf16[256,256]{1,0:T(8,128)(2,1)} %routed_layer.1) | data formatting | bytes 262144

commit v3 on v2

--- a/solution.py
+++ b/solution.py
@@ -97,28 +97,32 @@
 SOURCES = ((3, 2, 1), (0, 3, 2), (3, 0, 1), (0, 1, 2))
 TARGETS = ((3, 1, 2), (0, 3, 2), (3, 0, 1), (0, 2, 1))
 SCHEDULE = (
-    "N", "G10", "H01", "G11", "D", "G20", "H00", "G21", "H02", "Y1", "C1", "X1", "G31",
-    "S1", "G30", "X2", "C2", "P00", "Y2", "L1", "P01", "A00", "C3", "H12", "Y3", "H10",
-    "S2", "X3", "H11", "L2", "A01", "S3", "P10", "P11", "H22", "A10", "H21", "A11",
-    "F0", "L3", "H20", "E0", "P20", "H30", "E1", "P21", "A20", "H32", "A21", "H31",
-    "P30", "F1", "P31", "J0", "I1", "E2", "A30", "F2", "A31", "J1", "I0", "E3", "I2",
-    "F3", "J2", "I3", "J3", "R1", "R2", "R3",
+    "N", "D", "G10", "H00", "G11", "G20", "K2", "H02", "G21", "C1", "H01", "X1", "Y1",
+    "G31", "P00", "S1", "X2", "P01", "G30", "L1", "Y2", "C2", "S2", "A00", "Y3", "H11",
+    "H10", "X3", "H12", "L2", "C3", "A01", "P10", "P11", "S3", "H22", "A10", "H20",
+    "L3", "E0", "A11", "F0", "H21", "P20", "H32", "P21", "E1", "A20", "H30", "A21",
+    "H31", "P30", "F1", "P31", "E2", "J0", "A30", "F2", "I1", "K3", "A31", "J1", "I2",
+    "E3", "K1", "F3", "J2", "I3", "I0", "J3", "R1", "R2", "R3",
 )
 
 
 def fused_kernel(
-    tok_ref,
-    gain_ref,
-    ids_ref,
-    rw_ref,
+    tok_hbm,
+    gain_hbm,
+    ids_hbm,
+    rw_hbm,
     gw_hbm,
     uw_hbm,
     dw_hbm,
     dg_hbm,
     du_hbm,
     dd_hbm,
-    dgate_ref,
+    dgate_hbm,
     out_ref,
+    tok_ref,
+    gain_ref,
+    ids_ref,
+    rw_ref,
     gw,
     uw,
     dw,
@@ -149,6 +153,8 @@
     r2b_c,
     fin,
     ret,
+    chosen,
+    scale_col,
     total,
     wsem,
     zsem,
@@ -191,6 +197,11 @@
         )
 
     loads = {
+        "ids": pltpu.make_async_copy(ids_hbm, ids_ref, wsem.at[6]),
+        "tok": pltpu.make_async_copy(tok_hbm, tok_ref, wsem.at[7]),
+        "gain": pltpu.make_async_copy(gain_hbm, gain_ref, wsem.at[8]),
+        "rw": pltpu.make_async_copy(rw_hbm, rw_ref, wsem.at[9]),
+        "dgate": pltpu.make_async_copy(dgate_hbm, gates.at[tp], wsem.at[10]),
         "g": pltpu.make_async_copy(gw_hbm.at[0], gw, wsem.at[0]),
         "u": pltpu.make_async_copy(uw_hbm.at[0], uw, wsem.at[1]),
         "dg": pltpu.make_async_copy(dg_hbm, dgu.at[:, pl.ds(0, dsp)], wsem.at[2]),
@@ -257,12 +268,7 @@
     def span(slice_no):
         return pl.ds(pl.multiple_of(slice_no * cols, cols), cols)
 
-    step = 64
-    for i in range(0, group, step):
-        values = tok_ref[i : i + step, :].astype(F32)
-        mean = jnp.sum(values * values, axis=1, keepdims=True) * (1.0 / width)
-        factor[i : i + step, :] = jnp.broadcast_to(lax.rsqrt(mean + EPSILON), (step, 128))
-
+    need("ids")
     id0, id1 = ids_ref[0:1, :], ids_ref[1:2, :]
     number = lax.broadcasted_iota(jnp.int32, (128, group), 0)
     named = (id0 == number) | (id1 == number)
@@ -277,13 +283,20 @@
     slots = jnp.where(named, count, -1.0)
     slot_row[...] = slots
 
+    need("tok")
+    step = 64
+    for i in range(0, group, step):
+        values = tok_ref[i : i + step, :].astype(F32)
+        mean = jnp.sum(values * values, axis=1, keepdims=True) * (1.0 / width)
+        factor[i : i + step, :] = jnp.broadcast_to(lax.rsqrt(mean + EPSILON), (step, 128))
+
     def pick(e):
         row = slot_row[pl.ds(e, 1), :].astype(jnp.int32)
         where = lax.broadcasted_iota(jnp.int32, (cap, group), 0)
         return jnp.where(row == where, 1.0, 0.0).astype(BF)
 
+    need("gain")
     own = (tok_ref[:, span(tp)].astype(F32) * factor[:, 0:1] * gain_ref[:, span(tp)]).astype(BF)
-    gates[tp] = dgate_ref[...]
     for n in range(rounds):
         targets = [row[n] for row in TARGETS]
         plane = lookup(targets)
@@ -299,8 +312,9 @@
                 expected[kind, n + 1, h] = transfer(
                     src.at[n, rows], landed, sem.at[0, n, h], sem.at[1, n, h], at_tp(to_core)
                 )
+    need("dgate", "rw")
     for flip in range(1, 8):
-        send(("gate", flip), dgate_ref, gates.at[tp], at_tp(flip))
+        send(("gate", flip), gates.at[tp], gates.at[tp], at_tp(flip))
 
     weights = jnp.where(id0 == number, rw_ref[0:1, :], 0.0) + jnp.where(id1 == number, rw_ref[1:2, :], 0.0)
     slot_col[...] = slots.T
@@ -461,13 +475,21 @@
         mine = part[0, yy, xx, rows].astype(F32) + r0[yy, xx, rows].astype(F32)
         finish(b, 1, mine + r1b[xx].astype(F32) + r2b[...].astype(F32))
 
-    def returned(j):
+    def prepare(j):
         e = source(j)
         slot = jnp.sum(jnp.where(lane == e, slot_col[...], 0.0), axis=1, keepdims=True).astype(jnp.int32)
-        place = jnp.where(slot == lax.broadcasted_iota(jnp.int32, (group, cap), 1), 1.0, 0.0).astype(BF)
-        scale = weight_of(e)
+        where = lax.broadcasted_iota(jnp.int32, (group, cap), 1)
+        chosen[j - 1] = jnp.where(slot == where, 1.0, 0.0).astype(BF)
+        scale_col[j - 1] = jnp.broadcast_to(weight_of(e), (group, 128))
+
+    def returned(j):
         got(("r", j, 0), ("r", j, 1))
-        total[...] += scale * jnp.dot(place, ret[j - 1], preferred_element_type=F32)
+        rows = jnp.dot(chosen[j - 1], ret[j - 1], preferred_element_type=F32)
+        value = total[...] + scale_col[j - 1][:, 0:1] * rows
+        if ("R%d" % j) == SCHEDULE[-1]:
+            out_ref[...] = value.astype(BF)
+        else:
+            total[...] = value
 
     steps = {
         "N": norm_all,
@@ -485,11 +507,11 @@
         "F": scatter_two_b,
         "I": scatter_three_a,
         "J": scatter_three_b,
+        "K": prepare,
         "R": returned,
     }
     for word in SCHEDULE:
         steps[word[0]](*[int(digit) for digit in word[1:]])
-    out_ref[...] = total[...].astype(BF)
     for copy in started:
         copy.wait_send()
 
@@ -520,10 +542,14 @@
     half, ghalf = cap // 2, group // 2
     return pl.pallas_call(
         fused_kernel,
-        out_shape=jax.ShapeDtypeStruct((group, cols), BF),
-        in_specs=[vmem] * 4 + [hbm] * 6 + [vmem],
+        out_shape=pltpu.VMEM((group, cols), BF),
+        in_specs=[hbm] * 11,
         out_specs=vmem,
         scratch_shapes=[
+            pltpu.VMEM((group, width), BF),
+            pltpu.VMEM((1, width), F32),
+            pltpu.VMEM((2, group), jnp.int32),
+            pltpu.VMEM((2, group), F32),
             pltpu.VMEM((ffp, width), BF),
             pltpu.VMEM((ffp, width), BF),
             pltpu.VMEM((ffp, width), BF),
@@ -554,8 +580,10 @@
             pltpu.VMEM((rounds, half, cols), BF),
             pltpu.VMEM((rounds, cap, cols), BF),
             pltpu.VMEM((rounds, cap, cols), BF),
+            pltpu.VMEM((rounds, group, cap), BF),
+            pltpu.VMEM((rounds, group, 128), F32),
             pltpu.VMEM((group, cols), F32),
-            dma((6,)),
+            dma((11,)),
             dma((2, rounds, 2)),
             dma((2, rounds, 2)),
             dma((2, 92)),

time: 46.6 us -> 43.5 us (0.933)
  Pallas kernels: 44.9 us -> 42.6 us
  local copies, waits for them, and re-layouts: 1.57 us -> 0.66 us
    pallas_call x1, Pallas kernels: 44.9 us -> 42.6 us  [fused_local(): pl.pallas_call(fused_kernel, out_shape=pltpu.VMEM((group, cols), BF), in_...]
    unnamed x1, local copies, waits for them, and re-layouts: 1.57 us -> 0.66 us
where the time goes in v3:
time: 43.5 us; the launch traced here: 43.3 us
  Pallas kernels  42.6 us (98%)
  local copies, waits for them, and re-layouts  0.66 us (2%)
    pallas_call x1, Pallas kernels, fused_local(): pl.pallas_call(fused_kernel, out_shape=pltpu.VMEM((group, cols), BF), in_...  42.6 us

profile of v3, /device:TPU:0, one launch (start us, length us, event | category | flops | bytes accessed | tf_op | source)
XLA Modules:
  0.0 43.3 jit_solution(24761486684581319)
XLA Ops:
  0.0 42.6 %routed_layer.1 = bf16[256,256]{1,0:T(8,128)(2,1)S(1)} custom-call(bf16[256,2048]{1,0:T(8,128)(2,1)} %tok_hbm.1, f32[1,2048]{1,0:T(1,128)} %bitcast.8, s32[2,256]{1,0:T(2,128)} %bitcast.9, f32[2,256]{1,0:T(2,128)} %bitcast.10, bf16[1,704,2048]{2,1,0:T(8,128)(2,1)} %bitcast.6, bf16[1,704,2048]{2,1,0:T(8,128)(2,1)} %bitcast.7, bf16[1,704,2048]{2,1,0:T(8,128)(2,1)} %dw_hbm.1, ...), custom_call_target="tpu_custom_call" | custom-call | tf_op jit(solution)/shard_map/routed_layer/pallas_call | solution.py:543
  42.7 0.7 %copy.13 = bf16[256,256]{1,0:T(8,128)(2,1)} copy(bf16[256,256]{1,0:T(8,128)(2,1)S(1)} %routed_layer.1) | data formatting | bytes 262144

commit v4 on v3

--- a/solution.py
+++ b/solution.py
@@ -97,12 +97,11 @@
 SOURCES = ((3, 2, 1), (0, 3, 2), (3, 0, 1), (0, 1, 2))
 TARGETS = ((3, 1, 2), (0, 3, 2), (3, 0, 1), (0, 2, 1))
 SCHEDULE = (
-    "N", "D", "G10", "H00", "G11", "G20", "K2", "H02", "G21", "C1", "H01", "X1", "Y1",
-    "G31", "P00", "S1", "X2", "P01", "G30", "L1", "Y2", "C2", "S2", "A00", "Y3", "H11",
-    "H10", "X3", "H12", "L2", "C3", "A01", "P10", "P11", "S3", "H22", "A10", "H20",
-    "L3", "E0", "A11", "F0", "H21", "P20", "H32", "P21", "E1", "A20", "H30", "A21",
-    "H31", "P30", "F1", "P31", "E2", "J0", "A30", "F2", "I1", "K3", "A31", "J1", "I2",
-    "E3", "K1", "F3", "J2", "I3", "I0", "J3", "R1", "R2", "R3",
+    "N", "H0", "G10", "D", "G11", "G20", "G21", "X1", "W", "P00", "Y1", "C1", "P01",
+    "G31", "X2", "G30", "Y2", "S1", "C3", "L1", "A00", "S2", "H1", "C2", "Y3", "X3",
+    "L2", "P10", "K2", "S3", "K1", "P11", "A10", "A01", "H2", "L3", "P20", "A11", "P21",
+    "K3", "F1", "A20", "E1", "H3", "A21", "P30", "P31", "F2", "A30", "J1", "E2", "A31",
+    "I1", "J2", "F3", "E3", "E0", "F0", "I2", "J3", "I3", "J0", "I0", "R1", "R3", "R2",
 )
 
 
@@ -198,7 +197,6 @@
 
     loads = {
         "ids": pltpu.make_async_copy(ids_hbm, ids_ref, wsem.at[6]),
-        "tok": pltpu.make_async_copy(tok_hbm, tok_ref, wsem.at[7]),
         "gain": pltpu.make_async_copy(gain_hbm, gain_ref, wsem.at[8]),
         "rw": pltpu.make_async_copy(rw_hbm, rw_ref, wsem.at[9]),
         "dgate": pltpu.make_async_copy(dgate_hbm, gates.at[tp], wsem.at[10]),
@@ -209,6 +207,12 @@
         "d": pltpu.make_async_copy(dw_hbm.at[0], dw, wsem.at[4]),
         "dd": pltpu.make_async_copy(dd_hbm, dd, wsem.at[5]),
     }
+    step = group // 4
+    for i in range(4):
+        rows = pl.ds(i * step, step)
+        copy = pltpu.make_async_copy(tok_hbm.at[rows], tok_ref.at[rows], wsem.at[11 + i])
+        loads = {"tok%d" % i: copy, **loads}
+    loads = {"ids": loads.pop("ids"), **{"tok%d" % i: loads["tok%d" % i] for i in range(4)}, **loads}
     for load in loads.values():
         load.start()
 
@@ -268,27 +272,27 @@
     def span(slice_no):
         return pl.ds(pl.multiple_of(slice_no * cols, cols), cols)
 
-    need("ids")
-    id0, id1 = ids_ref[0:1, :], ids_ref[1:2, :]
     number = lax.broadcasted_iota(jnp.int32, (128, group), 0)
-    named = (id0 == number) | (id1 == number)
     earlier = jnp.where(
         lax.broadcasted_iota(jnp.int32, (group, group), 0)
         < lax.broadcasted_iota(jnp.int32, (group, group), 1),
         1.0,
         0.0,
     ).astype(BF)
+    need("ids")
+    id0, id1 = ids_ref[0:1, :], ids_ref[1:2, :]
+    named = (id0 == number) | (id1 == number)
     marks = jnp.where(named, 1.0, 0.0).astype(BF)
     count = jnp.dot(marks, earlier, preferred_element_type=F32)
     slots = jnp.where(named, count, -1.0)
     slot_row[...] = slots
 
-    need("tok")
-    step = 64
-    for i in range(0, group, step):
-        values = tok_ref[i : i + step, :].astype(F32)
+    for i in range(4):
+        need("tok%d" % i)
+        rows = pl.ds(i * step, step)
+        values = tok_ref[rows, :].astype(F32)
         mean = jnp.sum(values * values, axis=1, keepdims=True) * (1.0 / width)
-        factor[i : i + step, :] = jnp.broadcast_to(lax.rsqrt(mean + EPSILON), (step, 128))
+        factor[rows, :] = jnp.broadcast_to(lax.rsqrt(mean + EPSILON), (step, 128))
 
     def pick(e):
         row = slot_row[pl.ds(e, 1), :].astype(jnp.int32)
@@ -369,24 +373,24 @@
         got(("yx", j))
         forward("yxc", j, tops[1], 7, to_core)
 
-    tiles = [(n, min(256, ffp - n)) for n in range(0, ffp, 256)]
-
-    def hidden_tile(b, t):
+    def hidden(b):
         need("g", "u")
         if b:
             got(*[(name, b) for name in ("c", "xc", "yc", "xyc", "yxc")])
         rows = xbuf[b - 1] if b else normed[...]
-        n, size = tiles[t]
-        value = silu_mul(dot_t(rows, gw[n : n + size, :]), dot_t(rows, uw[n : n + size, :]))
+        value = silu_mul(dot_t(rows, gw[...]), dot_t(rows, uw[...]))
         if b:
-            hid_c[b - 1, :, n : n + size] = value
+            hid_c[b - 1] = value
         else:
-            hid_l[:, n : n + size] = value
+            hid_l[...] = value
+
+    def local_scale():
+        scale_col[rounds] = jnp.broadcast_to(weight_of(me), (group, 128))
 
     def dense_hidden():
         need("dg", "du")
-        acts = jnp.dot(normed[...], dgu[...], preferred_element_type=F32)
-        dhid[...] = silu_mul(acts[:, :dsp], acts[:, dsp:])
+        both = jnp.dot(normed[...], dgu[...], preferred_element_type=F32)
+        dhid[...] = silu_mul(both[:, :dsp], both[:, dsp:])
 
     def rs_refs(b):
         if b == 0:
@@ -403,7 +407,7 @@
         swap = half_no + (1 if b else 0)
         part, r0 = rs_refs(b)[:2]
         if b == 0:
-            scale = weight_of(me)
+            scale = scale_col[rounds][:, 0:1]
             got(*[("gate", flip) for flip in range(1, 8)])
         corners = ((1 - yy, 1 - xx), (yy, 1 - xx), (1 - yy, xx), (yy, xx))
         for (y, x), odd in zip(corners, (0, 1, 1, 0)):
@@ -499,7 +503,8 @@
         "Y": gather_relay_y,
         "S": gather_share,
         "L": gather_last,
-        "H": hidden_tile,
+        "H": hidden,
+        "W": local_scale,
         "D": dense_hidden,
         "P": partial,
         "A": scatter_one,
@@ -581,9 +586,9 @@
             pltpu.VMEM((rounds, cap, cols), BF),
             pltpu.VMEM((rounds, cap, cols), BF),
             pltpu.VMEM((rounds, group, cap), BF),
-            pltpu.VMEM((rounds, group, 128), F32),
+            pltpu.VMEM((rounds + 1, group, 128), F32),
             pltpu.VMEM((group, cols), F32),
-            dma((11,)),
+            dma((15,)),
             dma((2, rounds, 2)),
             dma((2, rounds, 2)),
             dma((2, 92)),

time: 43.5 us -> 43 us (0.989)
  Pallas kernels: 42.6 us -> 41.9 us
    pallas_call x1, Pallas kernels: 42.6 us -> 41.9 us  [fused_local(): pl.pallas_call(fused_kernel, out_shape=pltpu.VMEM((group, cols), BF), in_...]
where the time goes in v4:
time: 43 us; the launch traced here: 42.5 us
  Pallas kernels  41.9 us (97%)
  local copies, waits for them, and re-layouts  0.66 us (2%)
    pallas_call x1, Pallas kernels, fused_local(): pl.pallas_call(fused_kernel, out_shape=pltpu.VMEM((group, cols), BF), in_...  41.9 us

profile of v4, /device:TPU:0, one launch (start us, length us, event | category | flops | bytes accessed | tf_op | source)
XLA Modules:
  0.0 42.5 jit_solution(17284903725997085877)
XLA Ops:
  0.0 41.9 %routed_layer.1 = bf16[256,256]{1,0:T(8,128)(2,1)S(1)} custom-call(bf16[256,2048]{1,0:T(8,128)(2,1)} %tok_hbm.1, f32[1,2048]{1,0:T(1,128)} %bitcast.8, s32[2,256]{1,0:T(2,128)} %bitcast.9, f32[2,256]{1,0:T(2,128)} %bitcast.10, bf16[1,704,2048]{2,1,0:T(8,128)(2,1)} %bitcast.6, bf16[1,704,2048]{2,1,0:T(8,128)(2,1)} %bitcast.7, bf16[1,704,2048]{2,1,0:T(8,128)(2,1)} %dw_hbm.1, ...), custom_call_target="tpu_custom_call" | custom-call | tf_op jit(solution)/shard_map/routed_layer/pallas_call | solution.py:548
  41.9 0.7 %copy.13 = bf16[256,256]{1,0:T(8,128)(2,1)} copy(bf16[256,256]{1,0:T(8,128)(2,1)S(1)} %routed_layer.1) | data formatting | bytes 262144

commit v5 on v4

--- a/solution.py
+++ b/solution.py
@@ -94,14 +94,14 @@
     return lax.dot_general(rows, weights, (((1,), (1,)), ((), ())), preferred_element_type=F32)
 
 
-SOURCES = ((3, 2, 1), (0, 3, 2), (3, 0, 1), (0, 1, 2))
-TARGETS = ((3, 1, 2), (0, 3, 2), (3, 0, 1), (0, 2, 1))
+SOURCES = ((1, 2, 3), (3, 2, 0), (0, 1, 3), (2, 1, 0))
+TARGETS = ((2, 3, 1), (0, 2, 3), (3, 1, 0), (1, 0, 2))
 SCHEDULE = (
-    "N", "H0", "G10", "D", "G11", "G20", "G21", "X1", "W", "P00", "Y1", "C1", "P01",
-    "G31", "X2", "G30", "Y2", "S1", "C3", "L1", "A00", "S2", "H1", "C2", "Y3", "X3",
-    "L2", "P10", "K2", "S3", "K1", "P11", "A10", "A01", "H2", "L3", "P20", "A11", "P21",
-    "K3", "F1", "A20", "E1", "H3", "A21", "P30", "P31", "F2", "A30", "J1", "E2", "A31",
-    "I1", "J2", "F3", "E3", "E0", "F0", "I2", "J3", "I3", "J0", "I0", "R1", "R3", "R2",
+    "G10", "N", "G11", "H0", "X1", "C1", "D", "Y1", "G30", "W", "S1", "P00", "G31",
+    "K1", "P01", "L1", "G20", "K3", "X3", "Y3", "C3", "G21", "H1", "A00", "S3", "P10",
+    "K2", "X2", "L3", "C2", "P11", "Y2", "A10", "A11", "S2", "H3", "P30", "P31", "L2",
+    "F1", "E1", "A30", "A31", "H2", "P20", "J1", "P21", "E3", "I1", "A20", "F3", "A21",
+    "I3", "E2", "F2", "J3", "A01", "F0", "I2", "E0", "J2", "I0", "J0", "R3", "R1", "R2",
 )
 
 

time: 43 us -> 42.6 us (level)
  the two profiles are of different devices: /device:TPU:0 before, /device:TPU:11 now
where the time goes in v5:
time: 42.6 us; the launch traced here: 42.5 us
  Pallas kernels  41.8 us (98%)
  local copies, waits for them, and re-layouts  0.66 us (2%)
    pallas_call x1, Pallas kernels, fused_local(): pl.pallas_call(fused_kernel, out_shape=pltpu.VMEM((group, cols), BF), in_...  41.8 us

profile of v5, /device:TPU:11, one launch (start us, length us, event | category | flops | bytes accessed | tf_op | source)
XLA Modules:
  0.0 42.5 jit_solution(6404909622551674960)
XLA Ops:
  0.0 41.8 %routed_layer.1 = bf16[256,256]{1,0:T(8,128)(2,1)S(1)} custom-call(bf16[256,2048]{1,0:T(8,128)(2,1)} %tok_hbm.1, f32[1,2048]{1,0:T(1,128)} %bitcast.8, s32[2,256]{1,0:T(2,128)} %bitcast.9, f32[2,256]{1,0:T(2,128)} %bitcast.10, bf16[1,704,2048]{2,1,0:T(8,128)(2,1)} %bitcast.6, bf16[1,704,2048]{2,1,0:T(8,128)(2,1)} %bitcast.7, bf16[1,704,2048]{2,1,0:T(8,128)(2,1)} %dw_hbm.1, ...), custom_call_target="tpu_custom_call" | custom-call | tf_op jit(solution)/shard_map/routed_layer/pallas_call | solution.py:548
  41.8 0.7 %copy.13 = bf16[256,256]{1,0:T(8,128)(2,1)} copy(bf16[256,256]{1,0:T(8,128)(2,1)S(1)} %routed_layer.1) | data formatting | bytes 262144
